TPU v7x, 32 devices: a whole 2x2x4 slice. The times are simulated.
32 devices in a mesh: sp: 8 (over z, y), dp: 4 (over x, core).
Axes of the slice: x: 2, y: 2, z: 4, core: 2. Of those that a mesh axis runs over, the one named last changes fastest.
Arguments:
- query: bfloat16 [4, 1536, 3072], P('dp', 'sp'), may hold values from -18 to 18
- latent: bfloat16 [4, 1536, 1024], P('dp', 'sp'), may hold values from -6 to 6
- rope_key: bfloat16 [4, 1536, 32], P('dp', 'sp'), may hold values from -5 to 5
- latent_norm_gain: float32 [1024], replicated, may hold values from 0.1 to 1.9
- key_up_matrix: bfloat16 [2048, 1024], P('dp'), may hold values from -0.1875 to 0.1875
- value_up_matrix: bfloat16 [2048, 1024], P('dp'), may hold values from -0.1875 to 0.1875
- out_grad: bfloat16 [4, 1536, 2048], P('dp', 'sp'), may hold values from -6 to 6
Outputs:
- query_grad: bfloat16 [4, 1536, 3072], P('dp', 'sp')
- latent_grad: float32 [4, 1536, 1024], P('dp', 'sp')
- rope_key_grad: float32 [4, 1536, 32], P('dp', 'sp')
- key_weight_grad: float32 [2048, 1024], P('dp')
- value_weight_grad: float32 [2048, 1024], P('dp')
- gain_grad: float32 [1024], replicated
All inputs are finite; a program needn't handle non-finite values.
Results may differ from a plain program's by a relative error of at most 0.011.
Values may be sent and summed in bfloat16 or wider, within the bound.
A program may use at most 256 MiB of HBM per device.

v0:
```python
import jax
import jax.numpy as jnp
from jax import lax
from jax.sharding import PartitionSpec as P

ATTENTION_HEADS = 32
PLAIN_HEAD_WIDTH = 64
ROPE = 32
VALUE_HEAD_WIDTH = 64
SPAN = 64
eps = 1e-06
rope_base = 10000.0


def rotate(values, cosine, sine):
    half = values.shape[-1] // 2
    first = values[..., :half]
    second = values[..., half:]
    return jnp.concatenate(
        [first * cosine - second * sine, second * cosine + first * sine], axis=-1
    )


def angles(length, width):
    inverse = 1.0 / rope_base ** (jnp.arange(0, width, 2, dtype=jnp.float32) / width)
    turned = jnp.arange(length, dtype=jnp.float32)[:, None] * inverse[None, :]
    return (jnp.cos(turned), jnp.sin(turned))


def attend_backward(arrived, rope_full):
    f32 = jnp.float32
    bf16 = jnp.bfloat16
    length = arrived.shape[0]
    local_heads = arrived.shape[1]
    width = PLAIN_HEAD_WIDTH + ROPE
    scale = width ** (-0.5)
    block = 512
    cosine, sine = angles(length, ROPE)
    neg = jnp.finfo(f32).min
    q_nope = arrived[:, :, :PLAIN_HEAD_WIDTH]
    q_rope = rotate(
        arrived[:, :, PLAIN_HEAD_WIDTH:width].astype(f32), cosine[:, None, :], sine[:, None, :]
    ).astype(bf16)
    key_nope = arrived[:, :, width : width + PLAIN_HEAD_WIDTH]
    values = arrived[:, :, width + PLAIN_HEAD_WIDTH : width + PLAIN_HEAD_WIDTH + VALUE_HEAD_WIDTH]
    d_out = arrived[:, :, width + PLAIN_HEAD_WIDTH + VALUE_HEAD_WIDTH :]
    k_rope = rotate(rope_full.astype(f32), cosine, sine).astype(bf16)
    dk_nope = jnp.zeros((length, local_heads, PLAIN_HEAD_WIDTH), f32)
    dk_rope = jnp.zeros((length, ROPE), f32)
    d_vals = jnp.zeros((length, local_heads, VALUE_HEAD_WIDTH), f32)
    dq_parts = []
    for begin in range(0, length, block):
        end = begin + block
        qn = q_nope[begin:end]
        qr = q_rope[begin:end]
        go = d_out[begin:end]
        scores = jnp.einsum("qhd,khd->hqk", qn, key_nope[:end], preferred_element_type=f32)
        scores = (
            scores + jnp.einsum("qhd,kd->hqk", qr, k_rope[:end], preferred_element_type=f32)
        ) * scale
        q_seg = jnp.arange(begin, end) // SPAN
        k_seg = jnp.arange(end) // SPAN
        allowed = k_seg[None, :] <= q_seg[:, None]
        scores = jnp.where(allowed[None], scores, neg)
        probs = jax.nn.softmax(scores, axis=-1)
        d_probs = jnp.einsum("qhd,khd->hqk", go, values[:end], preferred_element_type=f32)
        d_scores = probs * (d_probs - jnp.sum(probs * d_probs, axis=-1, keepdims=True))
        ds_b = d_scores.astype(bf16)
        p_b = probs.astype(bf16)
        dq_n = jnp.einsum("hqk,khd->qhd", ds_b, key_nope[:end], preferred_element_type=f32) * scale
        dq_r = jnp.einsum("hqk,kd->qhd", ds_b, k_rope[:end], preferred_element_type=f32) * scale
        dq_r = rotate(dq_r, cosine[begin:end, None, :], -sine[begin:end, None, :])
        dq_parts.append(jnp.concatenate([dq_n, dq_r], axis=-1).astype(bf16))
        dk_nope = dk_nope.at[:end].add(
            jnp.einsum("hqk,qhd->khd", ds_b, qn, preferred_element_type=f32) * scale
        )
        dk_rope = dk_rope.at[:end].add(
            jnp.einsum("hqk,qhd->kd", ds_b, qr, preferred_element_type=f32) * scale
        )
        d_vals = d_vals.at[:end].add(
            jnp.einsum("hqk,qhd->khd", p_b, go, preferred_element_type=f32)
        )
    query_part = jnp.concatenate(dq_parts, axis=0)
    grads = jnp.concatenate([query_part, dk_nope.astype(bf16), d_vals.astype(bf16)], axis=-1)
    return (grads, rotate(dk_rope, cosine, -sine))


def local(query, latent, rope_key, latent_norm_gain, key_up_matrix, value_up_matrix, out_grad):
    f32 = jnp.float32
    bf16 = jnp.bfloat16
    tokens = latent.shape[1]
    width = PLAIN_HEAD_WIDTH + ROPE
    head_cols = ATTENTION_HEADS * PLAIN_HEAD_WIDTH
    lat = latent[0].astype(f32)
    inv_rms = lax.rsqrt(jnp.mean(lat * lat, axis=-1, keepdims=True) + eps)
    normed = lat * inv_rms
    nlat = (normed * latent_norm_gain).astype(bf16)
    stacked = jnp.stack([key_up_matrix, value_up_matrix])
    whole = lax.all_gather(stacked, "dp", axis=1, tiled=True)
    kv_tok = jnp.einsum("tc,gnc->tgn", nlat, whole, preferred_element_type=f32).astype(bf16)
    heads_query = query[0].reshape(tokens, ATTENTION_HEADS, width)
    key_nope = kv_tok[:, 0].reshape(tokens, ATTENTION_HEADS, PLAIN_HEAD_WIDTH)
    values = kv_tok[:, 1].reshape(tokens, ATTENTION_HEADS, VALUE_HEAD_WIDTH)
    d_out = out_grad[0].reshape(tokens, ATTENTION_HEADS, VALUE_HEAD_WIDTH)
    packed = jnp.concatenate([heads_query, key_nope, values, d_out], axis=2)
    arrived = lax.all_to_all(packed, "sp", split_axis=1, concat_axis=0, tiled=True)
    rope_full = lax.all_gather(rope_key[0], "sp", axis=0, tiled=True)
    grads_heads, rope_full_grad = attend_backward(arrived, rope_full)
    returned = lax.all_to_all(grads_heads, "sp", split_axis=0, concat_axis=1, tiled=True)
    rope_grad = lax.psum_scatter(rope_full_grad, "sp", scatter_dimension=0, tiled=True)
    query_grad = returned[:, :, :width].reshape(tokens, ATTENTION_HEADS * width)
    key_cols = returned[:, :, width : width + PLAIN_HEAD_WIDTH].reshape(tokens, head_cols)
    value_cols = returned[:, :, width + PLAIN_HEAD_WIDTH :].reshape(tokens, head_cols)
    dkv = jnp.stack([key_cols, value_cols], axis=1)
    d_nlat = jnp.einsum("tgn,gnc->tc", dkv, whole, preferred_element_type=f32)
    latents_all = lax.all_gather(nlat[None], "dp", axis=0, tiled=True)
    columns = lax.all_to_all(dkv[None], "dp", split_axis=3, concat_axis=0, tiled=True)
    partial_value = jnp.einsum("stgr,stc->grc", columns, latents_all, preferred_element_type=f32)
    weight_grads = lax.psum(partial_value, "sp")
    gain_grad = lax.psum(jnp.sum(d_nlat * normed, axis=0), ("sp", "dp"))
    scaled = d_nlat * latent_norm_gain
    latent_grad = inv_rms * (scaled - normed * jnp.mean(scaled * normed, axis=-1, keepdims=True))
    return (
        query_grad[None],
        latent_grad[None],
        rope_grad[None],
        weight_grads[0],
        weight_grads[1],
        gain_grad,
    )


def solution(mesh):
    in_specs = (
        P("dp", "sp", None),
        P("dp", "sp", None),
        P("dp", "sp", None),
        P(),
        P("dp", None),
        P("dp", None),
        P("dp", "sp", None),
    )
    out_specs = (
        P("dp", "sp", None),
        P("dp", "sp", None),
        P("dp", "sp", None),
        P("dp", None),
        P("dp", None),
        P(),
    )
    return jax.shard_map(local, mesh=mesh, in_specs=in_specs, out_specs=out_specs, check_vma=False)
```

profile of v0, /device:TPU:0, one launch (start us, length us, event | category | flops | bytes accessed | tf_op | source)
XLA Modules:
  0.0 738.0 jit_solution(6265751976223707838)
XLA Ops:
  16.4 55.1 %all-gather.4.cloned.1.call-done = bf16[2,2048,1024]{2,1,0:T(8,128)(2,1)} async-done(((bf16[2,512,1024]{2,1,0:T(8,128)(2,1)}), bf16[2,2048,1024]{2,1,0:T(8,128)(2,1)}) %all-gather.4.cloned.1.call-update) | async-done | bytes 8388624 | tf_op jit(solution)/shard_map/all_gather | solution.py:99
  71.5 6.2 convolution_convert_fusion
  87.8 5.6 pad_maximum_fusion
  97.4 5.6 all-to-all-start
  103.2 126.8 %all-gather = bf16[1,1536,32]{2,0,1:T(2,128)(2,1)S(1)} all-gather(bf16[1,192,32]{2,0,1:T(2,128)(2,1)S(1)} %copy.99), channel_id=2, replica_groups=mesh['sp'=8,'dp'=4] {'sp'}, dimensions={1}, use_global_device_ids=true | all-gather | bytes 110592 | tf_op jit(solution)/shard_map/all_gather | solution.py:107
  236.4 8.3 %copy.98 = bf16[8,192,4,288]{1,0,3,2:T(8,128)(2,1)} copy(bf16[8,192,4,288]{3,1,2,0:T(8,128)(2,1)} %bitcast.8) | data formatting | bytes 7077888 | tf_op jit(solution)/shard_map/all_to_all | solution.py:106
  244.7 6.9 all_to_all.42
  283.7 9.7 %multiply_convert_fusion.1 = bf16[4,512,1024]{2,1,0:T(8,128)(2,1)S(1)} fusion(f32[4,512,1024]{2,1,0:T(8,128)S(1)} %get-tuple-element.177, f32[4,512]{1,0:T(4,128)S(1)} %get-tuple-element.176, f32[4,512,1024]{2,1,0:T(8,128)S(1)} %get-tuple-element.171, f32[4,512]{1,0:T(4,128)S(1)} %get-tuple-element.170), kind=kLoop, calls=%fused_computation.12 | loop fusion | flops 8388608 | bytes 20987904 | tf_op jit(solution)/shard_map/convert_element_type | solution.py:68
  300.5 8.5 %fusion.4 = f32[4,512,1536]{2,1,0:T(8,128)} fusion(f32[1536,512,4]{0,1,2:T(8,128)S(1)} %fusion.114, pred[512,1536]{1,0:T(8,128)(4,1)S(1)} %copy-done.13, bf16[1536,4,288]{0,2,1:T(8,128)(2,1)} %copy-done.3), kind=kOutput, calls=%fused_computation.5 | convolution fusion | flops 412090368 | bytes 27000832 | tf_op jit(solution)/shard_map/qhd,khd->hqk/dot_general | solution.py:57
  309.1 14.9 %fusion.154 = (f32[4,512]{1,0:T(4,128)S(1)}, f32[4,512,1536]{2,1,0:T(8,128)}) fusion(f32[4,512,1536]{2,1,0:T(8,128)} %fusion.4), kind=kOutput, calls=%fused_computation.226 | output fusion | flops 6292991 | bytes 25174016 | tf_op jit(solution)/shard_map/sub | solution.py:65
  323.9 11.8 %multiply_reduce_fusion = (f32[4,512]{1,0:T(4,128)S(1)}, f32[4,512,1536]{2,1,0:T(8,128)}) fusion(f32[4,512,1536]{2,1,0:T(8,128)} %get-tuple-element.173, f32[4,512]{1,0:T(4,128)S(1)} %get-tuple-element.172, bf16[1536,4,288]{0,2,1:T(8,128)(2,1)} %copy-done.3), kind=kOutput, calls=%fused_computation.7 | convolution fusion | flops 412088320 | bytes 26230784 | tf_op jit(solution)/shard_map/qhd,khd->hqk/dot_general | solution.py:66
  335.7 6.0 multiply_convert_fusion
  351.6 11.2 %fusion.37 = f32[1536,4,64]{0,2,1:T(8,128)} fusion(f32[1536,4,64]{0,2,1:T(8,128)} %scatter-add.24, bf16[1536,4,288]{0,2,1:T(8,128)(2,1)} %copy-done.3, f32[4,512]{1,0:T(4,128)S(1)} %get-tuple-element.170, f32[4,512,1024]{2,1,0:T(8,128)} %copy-done.2), kind=kOutput, calls=%fused_computation.53 | convolution fusion | flops 274992128 | bytes 19144704 | tf_op jit(solution)/shard_map/hqk,qhd->khd/dot_general | solution.py:81
  367.2 13.7 %fusion.22 = bf16[1536,4,64]{0,2,1:T(8,128)(2,1)} fusion(f32[1536,4,64]{0,2,1:T(8,128)} %fusion.37, bf16[1536,4,288]{0,2,1:T(8,128)(2,1)} %copy-done.3, f32[4,512]{1,0:T(4,128)S(1)} %get-tuple-element.172, f32[4,512,1536]{2,1,0:T(8,128)} %fusion.4), kind=kOutput, calls=%fused_computation.36 | convolution fusion | flops 412880384 | bytes 27795456 | tf_op jit(solution)/shard_map/hqk,qhd->khd/dot_general | solution.py:81
  388.8 5.8 copy.107
  401.9 64.4 %all-to-all-done.1 = bf16[1536,4,224]{2,1,0:T(4,128)(2,1)} async-done(((bf16[1536,4,224]{2,1,0:T(4,128)(2,1)}), bf16[1536,4,224]{2,1,0:T(4,128)(2,1)}, u32[]{:S(2)}, u32[]{:S(2)}) %all-to-all-start.1) | async-done | bytes 2752544 | tf_op jit(solution)/shard_map/all_to_all | solution.py:109
  483.8 6.1 copy.116
  503.7 16.3 %all-to-all-done.2 = bf16[1,192,2,2048]{1,2,0,3:T(2,128)(2,1)} async-done(((bf16[1,192,2,2048]{1,2,0,3:T(2,128)(2,1)}), bf16[1,192,2,2048]{1,2,0,3:T(2,128)(2,1)}, u32[]{:S(2)}, u32[]{:S(2)}) %all-to-all-start.2) | async-done | bytes 1572896 | tf_op jit(solution)/shard_map/all_to_all | solution.py:117
  520.0 6.0 copy.118
  526.0 5.7 convolution_bitcast_fusion.1
  531.7 34.6 %reduce-scatter.4.cloned.1.call-done = f32[192,32]{1,0:T(8,128)} async-done(((f32[1536,32]{1,0:T(8,128)}), f32[192,32]{1,0:T(8,128)}) %reduce-scatter.4.cloned.1.call-update) | async-done | bytes 24592
  572.2 6.3 fusion.72
  578.5 44.0 %psum.15 = f32[1024]{0:T(1024)} all-reduce(f32[1024]{0:T(1024)S(1)} %get-tuple-element.138), channel_id=1, replica_groups=mesh['sp'=8,'dp'=4] {'sp','dp'}, use_global_device_ids=true, to_apply=%region_14.15 | all-reduce | flops 1024 | bytes 8192 | tf_op jit(solution)/shard_map/psum | solution.py:120
  623.6 102.6 %all-reduce.5.cloned.1.call-done = f32[2,512,1024]{2,1,0:T(8,128)} async-done(((f32[2,512,1024]{2,1,0:T(8,128)}), f32[2,512,1024]{2,1,0:T(8,128)}) %all-reduce.5.cloned.1.call-update) | async-done | bytes 4194320 | tf_op jit(solution)/shard_map/psum | solution.py:119
  (192 shorter events, 140.9 us)
Async XLA Ops:
  7.2 64.3 %all-gather.4.cloned.1.call-start = ((), (), s32[]{:S(2)}) async-start(), calls=%async_computation.4 | async-start | bytes 10485760 | tf_op jit(solution)/shard_map/all_gather | solution.py:99
  10.3 5.9 copy-start.10
  10.4 61.1 %copy-start.41 = (f32[1024]{0:T(1024)S(1)}, f32[1024]{0:T(1024)}, u32[]{:S(2)}) copy-start(f32[1024]{0:T(1024)} %param.34) | copy-start | bytes 12292
  16.4 55.1 %copy-start.44 = (f32[192]{0:T(256)}, f32[192]{0:T(256)S(1)}, u32[]{:S(2)}) copy-start(f32[192]{0:T(256)S(1)} %add_rsqrt_fusion) | copy-start | bytes 2308
  97.4 5.7 copy-start.43
  97.4 139.0 %all-to-all-start = ((bf16[192,32,288]{2,0,1:T(8,128)(2,1)}), bf16[192,32,288]{2,0,1:T(8,128)(2,1)}, u32[]{:S(2)}, u32[]{:S(2)}) async-start(bf16[192,32,288]{2,0,1:T(8,128)(2,1)} %copy.97), calls=%async_computation | async-start | bytes 9437184 | tf_op jit(solution)/shard_map/all_to_all | solution.py:106
  251.6 11.8 %copy-start.3 = (bf16[1536,4,288]{0,2,1:T(8,128)(2,1)}, bf16[1536,4,288]{0,2,1:T(8,128)(2,1)S(1)}, u32[]{:S(2)}) copy-start(bf16[1536,4,288]{0,2,1:T(8,128)(2,1)S(1)} %all_to_all.42) | copy-start | bytes 10616836
  268.0 5.0 copy-start.7
  268.0 5.0 copy-start.9
  293.4 5.2 copy-start.1
  323.9 11.8 %slice-start = ((s8[12582912]{0:T(1024)(128)(4,1)}), s8[4194304]{0:T(1024)(128)(4,1)S(1)}, s32[]{:S(2)}) async-start(s8[12582912]{0:T(1024)(128)(4,1)} %bitcast.187), calls=%async_computation.8 | async-start | bytes 8388608
  323.9 11.8 %slice-start.1 = ((s8[12582912]{0:T(1024)(128)(4,1)}), s8[4194304]{0:T(1024)(128)(4,1)S(1)}, s32[]{:S(2)}) async-start(s8[12582912]{0:T(1024)(128)(4,1)} %bitcast.187), calls=%async_computation.9 | async-start | bytes 8388608
  323.9 11.8 %slice-start.2 = ((s8[12582912]{0:T(1024)(128)(4,1)}), s8[4194304]{0:T(1024)(128)(4,1)S(1)}, s32[]{:S(2)}) async-start(s8[12582912]{0:T(1024)(128)(4,1)} %bitcast.187), calls=%async_computation.10 | async-start | bytes 8388608
  341.8 7.1 copy-start
  380.9 4.9 copy-start.25
  381.0 4.9 copy-start.26
  381.0 4.9 copy-start.27
  381.0 4.9 copy-start.33
  394.6 4.9 copy-start.45
  394.6 71.6 %all-to-all-start.1 = ((bf16[1536,4,224]{2,1,0:T(4,128)(2,1)}), bf16[1536,4,224]{2,1,0:T(4,128)(2,1)}, u32[]{:S(2)}, u32[]{:S(2)}) async-start(bf16[1536,4,224]{2,1,0:T(4,128)(2,1)} %copy.107), calls=%async_computation.1 | async-start | bytes 6291456 | tf_op jit(solution)/shard_map/all_to_all | solution.py:109
  399.2 126.8 %all-gather.6.cloned.1.call-start = ((), (), s32[]{:S(2)}) async-start(), calls=%async_computation.5 | async-start | bytes 1966080 | tf_op jit(solution)/shard_map/all_gather | solution.py:116
  489.8 30.2 %all-to-all-start.2 = ((bf16[1,192,2,2048]{1,2,0,3:T(2,128)(2,1)}), bf16[1,192,2,2048]{1,2,0,3:T(2,128)(2,1)}, u32[]{:S(2)}, u32[]{:S(2)}) async-start(bf16[1,192,2,2048]{1,2,0,3:T(2,128)(2,1)} %copy.116), calls=%async_computation.2 | async-start | bytes 4194304 | tf_op jit(solution)/shard_map/all_to_all | solution.py:117
  494.3 72.0 %reduce-scatter.4.cloned.1.call-start = ((), (), s32[]{:S(2)}) async-start(), calls=%async_computation.7 | async-start | bytes 884736
  503.6 222.6 %all-reduce.5.cloned.1.call-start = ((), (), s32[]{:S(2)}) async-start(), calls=%async_computation.6 | async-start | bytes 8388608 | tf_op jit(solution)/shard_map/psum | solution.py:119
  (34 other events, 102.9 us)
Sparse Core Ops, SparseCore 0:
  10.5 60.9 all-gather.3
  401.6 19.9 all-gather.5
  503.8 62.4 reduce-scatter.3
  569.8 156.3 all-reduce.4
where the time goes:
time: 747 us; the launch traced here: 738 us
  waiting for transfers between devices  273 us (37%)
  blocking collectives  171 us (23%)
  matrix products  118 us (16%)
  local copies, waits for them, and re-layouts  87 us (12%)
  other arithmetic  59.6 us (8%)
  starting transfers between devices  15.1 us (2%)
  between operations  15 us (2%)
    all_gather x1, blocking collectives, local(): rope_full = lax.all_gather(rope_key[0], 'sp', axis=0, tiled=True)  127 us
    psum x1, waiting for transfers between devices, local(): weight_grads = lax.psum(partial_value, 'sp')  103 us
    all_to_all x1, waiting for transfers between devices, local(): lax.all_to_all(grads_heads, 'sp', split_axis=0, concat_axis=1, tiled=True)  64.4 us
    all_gather x1, waiting for transfers between devices, local(): whole = lax.all_gather(stacked, 'dp', axis=1, tiled=True)  55.1 us
    psum x1, blocking collectives, local(): gain_grad = lax.psum(jnp.sum(d_nlat * normed, axis=0), ('sp', 'dp'))  44 us
    unnamed x5, waiting for transfers between devices  34.6 us
    dot_general x3, matrix products, attend_backward(): jnp.einsum('hqk,qhd->khd', p_b, go, preferred_element_type=f32)  30.3 us
    sub x3, other arithmetic, attend_backward(): probs = jax.nn.softmax(scores, axis=-1)  20.1 us
  transfers between devices with their start and end apart: 7, of which 5 were waited for; matrix products, arithmetic and copies ran while one was open for 10% of the time, Pallas kernels for 0%

commit v1 on v0

--- a/solution.py
+++ b/solution.py
@@ -116,7 +116,7 @@
     latents_all = lax.all_gather(nlat[None], "dp", axis=0, tiled=True)
     columns = lax.all_to_all(dkv[None], "dp", split_axis=3, concat_axis=0, tiled=True)
     partial_value = jnp.einsum("stgr,stc->grc", columns, latents_all, preferred_element_type=f32)
-    weight_grads = lax.psum(partial_value, "sp")
+    weight_grads = jnp.sum(lax.all_gather(partial_value, "sp"), axis=0)
     gain_grad = lax.psum(jnp.sum(d_nlat * normed, axis=0), ("sp", "dp"))
     scaled = d_nlat * latent_norm_gain
     latent_grad = inv_rms * (scaled - normed * jnp.mean(scaled * normed, axis=-1, keepdims=True))

time: 747 us -> 1240 us (1.66)
  waiting for transfers between devices: 273 us -> 716 us
  blocking collectives: 171 us -> 208 us
  other arithmetic: 59.6 us -> 74.4 us
    all_gather x0 -> x1, waiting for transfers between devices: none -> 546 us  [local(): weight_grads = jnp.sum(lax.all_gather(partial_value, 'sp'), axis=0)]
    psum x1 -> x0, waiting for transfers between devices: 103 us -> none  [local(): weight_grads = lax.psum(partial_value, 'sp')]
    psum x1, blocking collectives: 44 us -> 80.7 us  [local(): gain_grad = lax.psum(jnp.sum(d_nlat * normed, axis=0), ('sp', 'dp'))]
    reduce_sum x0 -> x1, other arithmetic: none -> 14.7 us  [local(): weight_grads = jnp.sum(lax.all_gather(partial_value, 'sp'), axis=0)]
  transfers between devices with their start and end apart: 7 -> 7, of which waited for: 5 -> 5; matrix products, arithmetic and copies ran while one was open for 10% -> 6% of each run, Pallas kernels for 0% -> 0%
where the time goes in v1:
time: 1240 us; the launch traced here: 1230 us
  waiting for transfers between devices  716 us (58%)
  blocking collectives  208 us (17%)
  matrix products  117 us (9%)
  local copies, waits for them, and re-layouts  86.9 us (7%)
  other arithmetic  74.4 us (6%)
  starting transfers between devices  15.1 us (1%)
  between operations  15 us (1%)
    all_gather x1, waiting for transfers between devices, local(): weight_grads = jnp.sum(lax.all_gather(partial_value, 'sp'), axis=0)  546 us
    all_gather x1, blocking collectives, local(): rope_full = lax.all_gather(rope_key[0], 'sp', axis=0, tiled=True)  127 us
    psum x1, blocking collectives, local(): gain_grad = lax.psum(jnp.sum(d_nlat * normed, axis=0), ('sp', 'dp'))  80.7 us
    all_to_all x1, waiting for transfers between devices, local(): lax.all_to_all(grads_heads, 'sp', split_axis=0, concat_axis=1, tiled=True)  64.4 us
    all_gather x1, waiting for transfers between devices, local(): whole = lax.all_gather(stacked, 'dp', axis=1, tiled=True)  55.1 us
    unnamed x5, waiting for transfers between devices  34.5 us
    dot_general x3, matrix products, attend_backward(): jnp.einsum('hqk,qhd->khd', p_b, go, preferred_element_type=f32)  30.2 us
  transfers between devices with their start and end apart: 7, of which 5 were waited for; matrix products, arithmetic and copies ran while one was open for 6% of the time, Pallas kernels for 0%

profile of v1, /device:TPU:0, one launch (start us, length us, event | category | flops | bytes accessed | tf_op | source)
XLA Modules:
  0.0 1232.3 jit_solution(11881398365884502534)
XLA Ops:
  16.4 55.1 %all-gather.6.cloned.1.call-done = bf16[2,2048,1024]{2,1,0:T(8,128)(2,1)} async-done(((bf16[2,512,1024]{2,1,0:T(8,128)(2,1)}), bf16[2,2048,1024]{2,1,0:T(8,128)(2,1)}) %all-gather.6.cloned.1.call-update) | async-done | bytes 8388624 | tf_op jit(solution)/shard_map/all_gather | solution.py:99
  71.5 6.2 convolution_convert_fusion
  97.4 5.6 all-to-all-start
  103.2 126.8 %all-gather = bf16[1,1536,32]{2,0,1:T(2,128)(2,1)S(1)} all-gather(bf16[1,192,32]{2,0,1:T(2,128)(2,1)S(1)} %copy.99), channel_id=2, replica_groups=mesh['sp'=8,'dp'=4] {'sp'}, dimensions={1}, use_global_device_ids=true | all-gather | bytes 110592 | tf_op jit(solution)/shard_map/all_gather | solution.py:107
  236.4 8.3 copy.98
  244.7 6.9 all_to_all.42
  283.6 9.7 multiply_convert_fusion.1
  300.5 8.5 fusion.4
  309.0 14.9 %fusion.154 = (f32[4,512]{1,0:T(4,128)S(1)}, f32[4,512,1536]{2,1,0:T(8,128)}) fusion(f32[4,512,1536]{2,1,0:T(8,128)} %fusion.4), kind=kOutput, calls=%fused_computation.226 | output fusion | flops 6292991 | bytes 25174016 | tf_op jit(solution)/shard_map/sub | solution.py:65
  323.9 11.8 multiply_reduce_fusion
  335.7 6.0 multiply_convert_fusion
  351.6 11.1 fusion.37
  367.1 13.7 %fusion.22 = bf16[1536,4,64]{0,2,1:T(8,128)(2,1)} fusion(f32[1536,4,64]{0,2,1:T(8,128)} %fusion.37, bf16[1536,4,288]{0,2,1:T(8,128)(2,1)} %copy-done.3, f32[4,512]{1,0:T(4,128)S(1)} %get-tuple-element.172, f32[4,512,1536]{2,1,0:T(8,128)} %fusion.4), kind=kOutput, calls=%fused_computation.36 | convolution fusion | flops 412880384 | bytes 27795456 | tf_op jit(solution)/shard_map/hqk,qhd->khd/dot_general | solution.py:81
  388.8 5.8 copy.107
  401.8 64.4 %all-to-all-done.1 = bf16[1536,4,224]{2,1,0:T(4,128)(2,1)} async-done(((bf16[1536,4,224]{2,1,0:T(4,128)(2,1)}), bf16[1536,4,224]{2,1,0:T(4,128)(2,1)}, u32[]{:S(2)}, u32[]{:S(2)}) %all-to-all-start.1) | async-done | bytes 2752544 | tf_op jit(solution)/shard_map/all_to_all | solution.py:109
  483.7 6.1 copy.116
  503.6 16.3 %all-to-all-done.2 = bf16[1,192,2,2048]{1,2,0,3:T(2,128)(2,1)} async-done(((bf16[1,192,2,2048]{1,2,0,3:T(2,128)(2,1)}), bf16[1,192,2,2048]{1,2,0,3:T(2,128)(2,1)}, u32[]{:S(2)}, u32[]{:S(2)}) %all-to-all-start.2) | async-done | bytes 1572896 | tf_op jit(solution)/shard_map/all_to_all | solution.py:117
  519.9 6.0 copy.118
  526.0 5.8 convolution_bitcast_fusion.1
  531.8 34.5 %reduce-scatter.4.cloned.1.call-done = f32[192,32]{1,0:T(8,128)} async-done(((f32[1536,32]{1,0:T(8,128)}), f32[192,32]{1,0:T(8,128)}) %reduce-scatter.4.cloned.1.call-update) | async-done | bytes 24592
  572.1 6.1 fusion.72
  578.3 80.7 %psum.7 = f32[1024]{0:T(1024)} all-reduce(f32[1024]{0:T(1024)S(1)} %get-tuple-element.138), channel_id=1, replica_groups=mesh['sp'=8,'dp'=4] {'sp','dp'}, use_global_device_ids=true, to_apply=%region_14.15 | all-reduce | flops 1024 | bytes 8192 | tf_op jit(solution)/shard_map/psum | solution.py:120
  660.1 545.7 %all-gather.10.cloned.1.call-done = f32[16,512,1024]{2,1,0:T(8,128)} async-done(((f32[2,512,1024]{2,1,0:T(8,128)}), f32[16,512,1024]{2,1,0:T(8,128)}) %all-gather.10.cloned.1.call-update) | async-done | bytes 33554448 | tf_op jit(solution)/shard_map/all_gather | solution.py:119
  1205.7 14.7 %reduce_sum.98 = f32[2,512,1024]{2,1,0:T(8,128)} reduce(f32[8,2,512,1024]{3,2,1,0:T(8,128)} %bitcast.190, f32[]{:T(128)} %constant.315.clone.1), dimensions={0}, to_apply=%region_12.13 | reduce | flops 7340032 | bytes 37748740 | tf_op jit(solution)/shard_map/reduce_sum | solution.py:119
  (193 shorter events, 146.5 us)
Async XLA Ops:
  7.2 64.3 %all-gather.6.cloned.1.call-start = ((), (), s32[]{:S(2)}) async-start(), calls=%async_computation.4 | async-start | bytes 10485760 | tf_op jit(solution)/shard_map/all_gather | solution.py:99
  10.3 5.9 copy-start.10
  10.4 61.1 %copy-start.41 = (f32[1024]{0:T(1024)S(1)}, f32[1024]{0:T(1024)}, u32[]{:S(2)}) copy-start(f32[1024]{0:T(1024)} %param.34) | copy-start | bytes 12292
  16.4 55.1 %copy-start.44 = (f32[192]{0:T(256)}, f32[192]{0:T(256)S(1)}, u32[]{:S(2)}) copy-start(f32[192]{0:T(256)S(1)} %add_rsqrt_fusion) | copy-start | bytes 2308
  97.4 5.7 copy-start.43
  97.4 139.0 %all-to-all-start = ((bf16[192,32,288]{2,0,1:T(8,128)(2,1)}), bf16[192,32,288]{2,0,1:T(8,128)(2,1)}, u32[]{:S(2)}, u32[]{:S(2)}) async-start(bf16[192,32,288]{2,0,1:T(8,128)(2,1)} %copy.97), calls=%async_computation | async-start | bytes 9437184 | tf_op jit(solution)/shard_map/all_to_all | solution.py:106
  251.6 11.8 copy-start.3
  268.0 5.0 copy-start.7
  268.0 5.0 copy-start.9
  293.4 5.2 copy-start.1
  323.9 11.8 slice-start
  323.9 11.8 slice-start.1
  323.9 11.8 slice-start.2
  341.8 7.1 copy-start
  380.9 4.9 copy-start.25
  380.9 4.9 copy-start.26
  380.9 4.9 copy-start.27
  380.9 4.9 copy-start.33
  394.5 4.9 copy-start.45
  394.6 71.6 %all-to-all-start.1 = ((bf16[1536,4,224]{2,1,0:T(4,128)(2,1)}), bf16[1536,4,224]{2,1,0:T(4,128)(2,1)}, u32[]{:S(2)}, u32[]{:S(2)}) async-start(bf16[1536,4,224]{2,1,0:T(4,128)(2,1)} %copy.107), calls=%async_computation.1 | async-start | bytes 6291456 | tf_op jit(solution)/shard_map/all_to_all | solution.py:109
  399.1 126.8 %all-gather.8.cloned.1.call-start = ((), (), s32[]{:S(2)}) async-start(), calls=%async_computation.5 | async-start | bytes 1966080 | tf_op jit(solution)/shard_map/all_gather | solution.py:116
  489.8 30.2 %all-to-all-start.2 = ((bf16[1,192,2,2048]{1,2,0,3:T(2,128)(2,1)}), bf16[1,192,2,2048]{1,2,0,3:T(2,128)(2,1)}, u32[]{:S(2)}, u32[]{:S(2)}) async-start(bf16[1,192,2,2048]{1,2,0,3:T(2,128)(2,1)} %copy.116), calls=%async_computation.2 | async-start | bytes 4194304 | tf_op jit(solution)/shard_map/all_to_all | solution.py:117
  494.2 72.0 %reduce-scatter.4.cloned.1.call-start = ((), (), s32[]{:S(2)}) async-start(), calls=%async_computation.7 | async-start | bytes 884736
  503.6 702.2 %all-gather.10.cloned.1.call-start = ((), (), s32[]{:S(2)}) async-start(), calls=%async_computation.6 | async-start | bytes 37748736 | tf_op jit(solution)/shard_map/all_gather | solution.py:119
  (34 other events, 102.8 us)
Sparse Core Ops, SparseCore 0:
  10.5 60.9 all-gather.5
  401.5 19.9 all-gather.7
  503.7 62.4 reduce-scatter.3
  567.6 638.0 all-gather.9
